TPU v7x, 32 devices: a whole 2x2x4 slice. The times are simulated.
32 devices in a mesh: fs: 4 (over y, x), tp: 8 (over z, core).
Axes of the slice: x: 2, y: 2, z: 4, core: 2. Of those that a mesh axis runs over, the one named last changes fastest.
Arguments:
- prompt: bfloat16 [4096, 2048], P(('fs', 'tp')), may hold values from -6 to 6
- norm_gain: float32 [2048], P('tp'), may hold values from 0.1 to 1.9
- gate_master: float32 [8, 2, 512, 2048], P(None, None, 'fs', 'tp'), may hold values from -0.125 to 0.125
- up_master: float32 [8, 2, 512, 2048], P(None, None, 'fs', 'tp'), may hold values from -0.125 to 0.125
- down_master: float32 [8, 2, 512, 2048], P(None, None, 'fs', 'tp'), may hold values from -0.25 to 0.25
- group_pick: int32 [4096, 1], P(('fs', 'tp')), may hold values from 0 to 7; in each aligned block of 128 rows (0 to 127, 128 to 255, ...) at most 32 rows name the same one
- route_weight: bfloat16 [4096, 2], P(('fs', 'tp')), may hold values from 0.099609375 to 1
Outputs:
- gate_serve: bfloat16 [8, 2, 512, 2048], P('tp', None, 'fs')
- up_serve: bfloat16 [8, 2, 512, 2048], P('tp', None, 'fs')
- down_serve: bfloat16 [8, 2, 512, 2048], P('tp', None, 'fs')
- mixed: bfloat16 [4096, 2048], P(('fs', 'tp'))
Inputs may be any that keep to these rules, and one draw needn't show every extreme that they name: `group_pick`: in the rows of one device no group is named by more than 32 rows, and in every draw some device's rows name one group exactly 32 times.
All inputs are finite; a program needn't handle non-finite values.
Results may differ from a plain program's by a relative error of at most 0.0081.
Values may be sent and summed in bfloat16 or wider, within the bound.
A program may use at most 64 MiB of HBM per device.

v0:
```python
import jax
import jax.numpy as jnp
from jax import lax
from jax.sharding import PartitionSpec as P

EPS = 1e-06


def expert_rows(group_rows, weights, pieces):
    gate_piece, up_piece, down_piece = pieces
    expert_count = gate_piece.shape[1]
    unit_count = gate_piece.shape[2]
    model_width = gate_piece.shape[3]
    row_count = group_rows.shape[0]
    gate_matrix = gate_piece.reshape(expert_count * unit_count, model_width)
    up_matrix = up_piece.reshape(expert_count * unit_count, model_width)
    down_matrix = down_piece.reshape(expert_count * unit_count, model_width)
    gate_pre = jnp.einsum("sd,hd->sh", group_rows, gate_matrix, preferred_element_type=jnp.float32)
    up_pre = jnp.einsum("sd,hd->sh", group_rows, up_matrix, preferred_element_type=jnp.float32)
    active = (jax.nn.silu(gate_pre) * up_pre).reshape(row_count, expert_count, unit_count)
    hidden = (weights.astype(jnp.float32)[:, :, None] * active).reshape(
        row_count, expert_count * unit_count
    )
    hidden = hidden.astype(jnp.bfloat16)
    return jnp.dot(hidden, down_matrix, preferred_element_type=jnp.float32)


def per_device(prompt, norm_gain, gate_master, up_master, down_master, group_pick, route_weight):
    group_total = lax.axis_size("tp")
    gate_local = (gate_master * norm_gain).astype(jnp.bfloat16)
    up_local = (up_master * norm_gain).astype(jnp.bfloat16)
    down_local = down_master.astype(jnp.bfloat16)
    gate_serve, up_serve, down_serve = (
        lax.all_to_all(gate_local, "tp", split_axis=0, concat_axis=3, tiled=True),
        lax.all_to_all(up_local, "tp", split_axis=0, concat_axis=3, tiled=True),
        lax.all_to_all(down_local, "tp", split_axis=0, concat_axis=3, tiled=True),
    )
    values = prompt.astype(jnp.float32)
    normed = (values * lax.rsqrt(jnp.mean(values * values, axis=1, keepdims=True) + EPS)).astype(
        jnp.bfloat16
    )
    tok_count = prompt.shape[0]
    capacity = 2 * tok_count // group_total
    slot_total = group_total * capacity
    chosen = group_pick[:, 0]
    member = (chosen[:, None] == jnp.arange(group_total, dtype=jnp.int32)[None, :]).astype(
        jnp.int32
    )
    slot_rank = jnp.sum(jnp.cumsum(member, axis=0) * member, axis=1) - 1
    target = chosen * capacity + slot_rank
    placing = (jnp.arange(slot_total, dtype=jnp.int32)[:, None] == target[None, :]).astype(
        jnp.bfloat16
    )
    send_rows = jnp.dot(placing, normed, preferred_element_type=jnp.float32).astype(jnp.bfloat16)
    send_weights = jnp.dot(placing, route_weight, preferred_element_type=jnp.float32).astype(
        jnp.bfloat16
    )
    got_rows, got_weights = (
        lax.all_to_all(
            send_rows.reshape(group_total, capacity, -1),
            "tp",
            split_axis=0,
            concat_axis=0,
            tiled=True,
        ),
        lax.all_to_all(
            send_weights.reshape(group_total, capacity, -1),
            "tp",
            split_axis=0,
            concat_axis=0,
            tiled=True,
        ),
    )
    group_rows = got_rows.reshape(slot_total, -1)
    weights = got_weights.reshape(slot_total, -1)
    gathered = (
        lax.all_gather(gate_serve, "fs", axis=2, tiled=True),
        lax.all_gather(up_serve, "fs", axis=2, tiled=True),
        lax.all_gather(down_serve, "fs", axis=2, tiled=True),
    )
    summed = expert_rows(group_rows, weights, gathered)
    result = summed.astype(jnp.bfloat16).reshape(group_total, capacity, -1)
    returned = lax.all_to_all(result, "tp", split_axis=0, concat_axis=0, tiled=True)
    mixed = jnp.einsum(
        "st,sd->td", placing, returned.reshape(slot_total, -1), preferred_element_type=jnp.float32
    ).astype(jnp.bfloat16)
    return (gate_serve, up_serve, down_serve, mixed)


def solution(mesh):
    placed = (
        P(("fs", "tp"), None),
        P("tp"),
        P(None, None, "fs", "tp"),
        P(None, None, "fs", "tp"),
        P(None, None, "fs", "tp"),
        P(("fs", "tp"), None),
        P(("fs", "tp"), None),
    )
    return jax.shard_map(
        per_device,
        mesh=mesh,
        in_specs=placed,
        out_specs=(
            P("tp", None, "fs", None),
            P("tp", None, "fs", None),
            P("tp", None, "fs", None),
            P(("fs", "tp"), None),
        ),
        check_vma=False,
    )
```

profile of v0, /device:TPU:0, one launch (start us, length us, event | category | flops | bytes accessed | tf_op | source)
XLA Modules:
  0.0 250.6 jit_solution(5716967491578532564)
XLA Ops:
  7.2 2.7 %multiply_convert_fusion = (bf16[8,2,128,256]{3,2,1,0:T(8,128)(2,1)S(1)}, bf16[8,2,128,256]{3,2,1,0:T(8,128)(2,1)S(1)}) fusion(f32[8,2,128,256]{3,2,1,0:T(8,128)} %param.10, f32[256]{0:T(256)} %param.8, f32[8,2,128,256]{3,2,1,0:T(8,128)} %param.9), kind=kLoop, calls=%fused_computation.3 | loop fusion | flops 2097152 | bytes 6292480 | tf_op jit(solution)/shard_map/convert_element_type | solution.py:31
  9.9 32.7 %all_to_all.69 = bf16[8,2,128,256]{3,2,1,0:T(8,128)(2,1)S(1)} all-to-all(bf16[8,2,128,256]{3,2,1,0:T(8,128)(2,1)S(1)} %get-tuple-element.5), channel_id=1, replica_groups=mesh['fs'=4,'tp'=8] {'tp'}, dimensions={0} | all-to-all | bytes 2097152 | tf_op jit(solution)/shard_map/all_to_all | solution.py:34
  42.7 1.1 copy.32
  43.8 29.0 %all_to_all.70 = bf16[8,2,128,256]{3,2,1,0:T(8,128)(2,1)S(1)} all-to-all(bf16[8,2,128,256]{3,2,1,0:T(8,128)(2,1)S(1)} %get-tuple-element.4), channel_id=1, replica_groups=mesh['fs'=4,'tp'=8] {'tp'}, dimensions={0} | all-to-all | bytes 2097152 | tf_op jit(solution)/shard_map/all_to_all | solution.py:35
  72.8 1.1 copy.33
  74.2 29.0 %all_to_all.71 = bf16[8,2,128,256]{3,2,1,0:T(8,128)(2,1)S(1)} all-to-all(bf16[8,2,128,256]{3,2,1,0:T(8,128)(2,1)S(1)} %convert_element_type.46), channel_id=1, replica_groups=mesh['fs'=4,'tp'=8] {'tp'}, dimensions={0} | all-to-all | bytes 2097152 | tf_op jit(solution)/shard_map/all_to_all | solution.py:36
  103.1 1.1 copy.34
  104.4 0.2 reduce_window_sum.11
  104.5 0.2 select_reduce_fusion
  105.0 0.6 copy.28
  105.6 3.3 %all-to-all-start.3 = ((bf16[8,32,2]{1,2,0:T(2,128)(2,1)}), bf16[8,32,2]{1,2,0:T(2,128)(2,1)S(1)}, u32[]{:S(2)}, u32[]{:S(2)}) async-start(bf16[8,32,2]{1,2,0:T(2,128)(2,1)} %copy.28), calls=%async_computation.3 | async-start | bytes 8192 | tf_op jit(solution)/shard_map/all_to_all | solution.py:66
  108.9 0.2 fusion.2
  109.1 1.6 convolution_convert_fusion
  110.7 3.7 %all-to-all-done.3 = bf16[8,32,2]{1,2,0:T(2,128)(2,1)S(1)} async-done(((bf16[8,32,2]{1,2,0:T(2,128)(2,1)}), bf16[8,32,2]{1,2,0:T(2,128)(2,1)S(1)}, u32[]{:S(2)}, u32[]{:S(2)}) %all-to-all-start.3) | async-done | bytes 1056 | tf_op jit(solution)/shard_map/all_to_all | solution.py:66
  114.3 3.6 %all-to-all-start.4 = ((bf16[8,32,2048]{2,1,0:T(8,128)(2,1)}), bf16[8,32,2048]{2,1,0:T(8,128)(2,1)S(1)}, u32[]{:S(2)}, u32[]{:S(2)}) async-start(bf16[8,32,2048]{2,1,0:T(8,128)(2,1)} %bitcast.8), calls=%async_computation.4 | async-start | bytes 2097152 | tf_op jit(solution)/shard_map/all_to_all | solution.py:59
  118.0 0.3 mul.62
  118.4 0.2 copy.35
  118.6 25.8 %all-to-all-done.4 = bf16[8,32,2048]{2,1,0:T(8,128)(2,1)S(1)} async-done(((bf16[8,32,2048]{2,1,0:T(8,128)(2,1)}), bf16[8,32,2048]{2,1,0:T(8,128)(2,1)S(1)}, u32[]{:S(2)}, u32[]{:S(2)}) %all-to-all-start.4) | async-done | bytes 1048608 | tf_op jit(solution)/shard_map/all_to_all | solution.py:59
  144.4 4.6 %fusion.12 = f32[256,1024]{1,0:T(8,128)} fusion(bf16[256,2048]{1,0:T(8,128)(2,1)S(1)} %bitcast.47, bf16[1024,2048]{1,0:T(8,128)(2,1)} %bitcast.54), kind=kOutput, calls=%fused_computation.26 | convolution fusion | flops 1073741824 | bytes 6291456 | tf_op jit(solution)/shard_map/sd,hd->sh/dot_general | solution.py:18
  149.0 1.4 all-gather.6.cloned.1.call-done
  150.5 55.0 %all-gather.8.cloned.1.call-done = bf16[1,2,512,2048]{3,2,1,0:T(8,128)(2,1)} async-done(((bf16[1,2,128,2048]{3,2,1,0:T(8,128)(2,1)}), bf16[1,2,512,2048]{3,2,1,0:T(8,128)(2,1)}) %all-gather.8.cloned.1.call-update) | async-done | bytes 4194320 | tf_op jit(solution)/shard_map/all_gather | solution.py:79
  205.5 6.4 %convolution_convert_fusion.1 = bf16[256,2048]{1,0:T(8,128)(2,1)S(1)} fusion(bf16[1024,2048]{1,0:T(8,128)(2,1)} %bitcast.56, f32[256,1024]{1,0:T(8,128)S(1)} %bitcast.49, bf16[256,2048]{1,0:T(8,128)(2,1)S(1)} %bitcast.48, bf16[1024,2048]{1,0:T(8,128)(2,1)} %bitcast.55, f32[256,1024]{1,0:T(8,128)} %fusion.12), kind=kOutput, calls=%fused_computation.1 | convolution fusion | flops 2149842944 | bytes 12582912 | tf_op jit(solution)/shard_map/dot_general | solution.py:25
  211.9 31.0 %all_to_all.72 = bf16[8,32,2048]{2,1,0:T(8,128)(2,1)S(1)} all-to-all(bf16[8,32,2048]{2,1,0:T(8,128)(2,1)S(1)} %bitcast.50), channel_id=1, replica_groups=mesh['fs'=4,'tp'=8] {'tp'}, dimensions={0} | all-to-all | bytes 2097152 | tf_op jit(solution)/shard_map/all_to_all | solution.py:83
  242.9 1.1 convolution_convert_fusion.2
  (23 shorter events, 0.8 us)
Async XLA Ops:
  7.2 97.6 %copy-start = (bf16[128,2]{0,1:T(2,128)(2,1)S(1)}, bf16[128,2]{0,1:T(2,128)(2,1)}, u32[]{:S(2)}) copy-start(bf16[128,2]{0,1:T(2,128)(2,1)} %param.13) | copy-start | bytes 1540
  7.2 137.2 %all-gather.4.cloned.1.call-start = ((), (), s32[]{:S(2)}) async-start(), calls=%async_computation.6 | async-start | bytes 5242880 | tf_op jit(solution)/shard_map/all_gather | solution.py:77
  42.7 31.4 %copy-start.1 = (f32[8,2,128,256]{3,2,1,0:T(8,128)S(1)}, f32[8,2,128,256]{3,2,1,0:T(8,128)}, u32[]{:S(2)}) copy-start(f32[8,2,128,256]{3,2,1,0:T(8,128)} %param.11) | copy-start | bytes 6291460
  43.8 106.7 %all-gather.6.cloned.1.call-start = ((), (), s32[]{:S(2)}) async-start(), calls=%async_computation.7 | async-start | bytes 5242880 | tf_op jit(solution)/shard_map/all_gather | solution.py:78
  73.9 30.3 %copy-start.3 = (s32[128,1]{0,1:T(1,128)S(1)}, s32[128,1]{0,1:T(1,128)}, u32[]{:S(2)}) copy-start(s32[128,1]{0,1:T(1,128)} %param.12) | copy-start | bytes 1540
  73.9 35.0 %copy-start.2 = (bf16[128,2048]{1,0:T(8,128)(2,1)S(1)}, bf16[128,2048]{1,0:T(8,128)(2,1)}, u32[]{:S(2)}) copy-start(bf16[128,2048]{1,0:T(8,128)(2,1)} %param.7) | copy-start | bytes 1572868
  74.0 131.5 %all-gather.8.cloned.1.call-start = ((), (), s32[]{:S(2)}) async-start(), calls=%async_computation.8 | async-start | bytes 5242880 | tf_op jit(solution)/shard_map/all_gather | solution.py:79
  105.6 8.8 %all-to-all-start.3 = ((bf16[8,32,2]{1,2,0:T(2,128)(2,1)}), bf16[8,32,2]{1,2,0:T(2,128)(2,1)S(1)}, u32[]{:S(2)}, u32[]{:S(2)}) async-start(bf16[8,32,2]{1,2,0:T(2,128)(2,1)} %copy.28), calls=%async_computation.3 | async-start | bytes 8192 | tf_op jit(solution)/shard_map/all_to_all | solution.py:66
  114.3 30.1 %all-to-all-start.4 = ((bf16[8,32,2048]{2,1,0:T(8,128)(2,1)}), bf16[8,32,2048]{2,1,0:T(8,128)(2,1)S(1)}, u32[]{:S(2)}, u32[]{:S(2)}) async-start(bf16[8,32,2048]{2,1,0:T(8,128)(2,1)} %bitcast.8), calls=%async_computation.4 | async-start | bytes 2097152 | tf_op jit(solution)/shard_map/all_to_all | solution.py:59
Sparse Core Ops, SparseCore 0:
  43.9 51.4 all-gather.3
  97.9 52.5 all-gather.5
  152.9 52.5 all-gather.7
where the time goes:
time: 251 us
  blocking collectives  122 us (49%)
  waiting for transfers between devices  86 us (34%)
  matrix products  13.9 us (6%)
  between operations  13.9 us (6%)
  starting transfers between devices  6.99 us (3%)
  local copies, waits for them, and re-layouts  4.69 us (2%)
  other arithmetic  3.46 us (1%)
    all_gather x1, waiting for transfers between devices, per_device(): lax.all_gather(down_serve, 'fs', axis=2, tiled=True)  55 us
    all_to_all x1, blocking collectives, per_device(): lax.all_to_all(gate_local, 'tp', split_axis=0, concat_axis=3, tiled=True)  32.7 us
    all_to_all x1, blocking collectives, per_device(): lax.all_to_all(result, 'tp', split_axis=0, concat_axis=0, tiled=True)  31 us
    all_to_all x1, blocking collectives, per_device(): lax.all_to_all(up_local, 'tp', split_axis=0, concat_axis=3, tiled=True)  29 us
    all_to_all x1, blocking collectives, per_device(): lax.all_to_all(down_local, 'tp', split_axis=0, concat_axis=3, tiled=True)  29 us
    all_to_all x1, waiting for transfers between devices, per_device(): lax.all_to_all(send_rows.reshape(group_total, capacity, -1), 'tp', split_...  25.8 us
    dot_general x1, matrix products, expert_rows(): return jnp.dot(hidden, down_matrix, preferred_element_type=jnp.float32)  6.42 us
  transfers between devices with their start and end apart: 5, of which 4 were waited for; matrix products, arithmetic and copies ran while one was open for 4% of the time, Pallas kernels for 0%

commit v1 on v0

--- a/solution.py
+++ b/solution.py
@@ -1,9 +1,25 @@
+import functools
 import jax
 import jax.numpy as jnp
 from jax import lax
 from jax.sharding import PartitionSpec as P
 
 EPS = 1e-06
+
+
+def state_kinds_on_mesh(field_in, axis_name, along_dim, dim_no):
+    return jnp.concatenate(
+        lax.all_to_all(
+            jnp.stack(jnp.split(field_in, lax.axis_size(axis_name), along_dim)),
+            axis_name=axis_name,
+            split_axis=0,
+            concat_axis=0,
+        ),
+        axis=dim_no,
+    )
+
+
+_arrange_matrix = functools.partial(state_kinds_on_mesh, axis_name="tp", along_dim=0, dim_no=3)
 
 
 def expert_rows(group_rows, weights, pieces):
@@ -33,7 +49,7 @@
     gate_serve, up_serve, down_serve = (
         lax.all_to_all(gate_local, "tp", split_axis=0, concat_axis=3, tiled=True),
         lax.all_to_all(up_local, "tp", split_axis=0, concat_axis=3, tiled=True),
-        lax.all_to_all(down_local, "tp", split_axis=0, concat_axis=3, tiled=True),
+        _arrange_matrix(down_local),
     )
     values = prompt.astype(jnp.float32)
     normed = (values * lax.rsqrt(jnp.mean(values * values, axis=1, keepdims=True) + EPS)).astype(

time: 251 us -> 251 us (level)
    all_gather x1, waiting for transfers between devices: 55 us -> 1.31 us  [per_device(): lax.all_gather(down_serve, 'fs', axis=2, tiled=True)]
    all_gather x1, waiting for transfers between devices: 1.44 us -> 55 us  [per_device(): lax.all_gather(up_serve, 'fs', axis=2, tiled=True)]
where the time goes in v1:
time: 251 us
  blocking collectives  122 us (49%)
  waiting for transfers between devices  85.9 us (34%)
  matrix products  13.9 us (6%)
  between operations  13.9 us (6%)
  starting transfers between devices  6.99 us (3%)
  local copies, waits for them, and re-layouts  4.77 us (2%)
  other arithmetic  3.41 us (1%)
    all_gather x1, waiting for transfers between devices, per_device(): lax.all_gather(up_serve, 'fs', axis=2, tiled=True)  55 us
    all_to_all x1, blocking collectives, per_device(): lax.all_to_all(gate_local, 'tp', split_axis=0, concat_axis=3, tiled=True)  32.8 us
    all_to_all x1, blocking collectives, per_device(): lax.all_to_all(result, 'tp', split_axis=0, concat_axis=0, tiled=True)  31 us
    all_to_all x1, blocking collectives, state_kinds_on_mesh(): lax.all_to_all(jnp.stack(jnp.split(field_in, lax.axis_size(axis_name), al...  29 us
    all_to_all x1, blocking collectives, per_device(): lax.all_to_all(up_local, 'tp', split_axis=0, concat_axis=3, tiled=True)  29 us
    all_to_all x1, waiting for transfers between devices, per_device(): lax.all_to_all(send_rows.reshape(group_total, capacity, -1), 'tp', split_...  25.8 us
    dot_general x1, matrix products, expert_rows(): return jnp.dot(hidden, down_matrix, preferred_element_type=jnp.float32)  6.43 us
  transfers between devices with their start and end apart: 5, of which 4 were waited for; matrix products, arithmetic and copies ran while one was open for 4% of the time, Pallas kernels for 0%

profile of v1, /device:TPU:0, one launch (start us, length us, event | category | flops | bytes accessed | tf_op | source)
XLA Modules:
  0.0 250.7 jit_solution(1576310928321932488)
XLA Ops:
  7.2 2.7 %multiply_convert_fusion = (bf16[8,2,128,256]{3,2,1,0:T(8,128)(2,1)S(1)}, bf16[8,2,128,256]{3,2,1,0:T(8,128)(2,1)S(1)}) fusion(f32[8,2,128,256]{3,2,1,0:T(8,128)} %param.10, f32[256]{0:T(256)} %param.8, f32[8,2,128,256]{3,2,1,0:T(8,128)} %param.9), kind=kLoop, calls=%fused_computation.3 | loop fusion | flops 2097152 | bytes 6292480 | tf_op jit(solution)/shard_map/convert_element_type | solution.py:47
  9.9 32.8 %all_to_all.56 = bf16[8,2,128,256]{3,2,1,0:T(8,128)(2,1)S(1)} all-to-all(bf16[8,2,128,256]{3,2,1,0:T(8,128)(2,1)S(1)} %get-tuple-element.5), channel_id=1, replica_groups=mesh['fs'=4,'tp'=8] {'tp'}, dimensions={0} | all-to-all | bytes 2097152 | tf_op jit(solution)/shard_map/all_to_all | solution.py:50
  42.7 1.1 copy.32
  44.2 29.0 %all_to_all.57 = bf16[8,1,2,128,256]{4,3,2,1,0:T(8,128)(2,1)S(1)} all-to-all(bf16[8,1,2,128,256]{4,3,2,1,0:T(8,128)(2,1)S(1)} %fusion.7), channel_id=1, replica_groups=mesh['fs'=4,'tp'=8] {'tp'}, dimensions={0} | all-to-all | bytes 2097152 | tf_op jit(solution)/shard_map/all_to_all | solution.py:12
  73.2 1.1 copy.34
  74.4 29.0 %all_to_all.58 = bf16[8,2,128,256]{3,2,1,0:T(8,128)(2,1)S(1)} all-to-all(bf16[8,2,128,256]{3,2,1,0:T(8,128)(2,1)S(1)} %get-tuple-element.4), channel_id=1, replica_groups=mesh['fs'=4,'tp'=8] {'tp'}, dimensions={0} | all-to-all | bytes 2097152 | tf_op jit(solution)/shard_map/all_to_all | solution.py:51
  103.4 1.1 copy.33
  104.6 0.2 reduce_window_sum.11
  104.8 0.2 select_reduce_fusion
  105.2 0.6 copy.28
  105.8 3.3 %all-to-all-start.3 = ((bf16[8,32,2]{1,2,0:T(2,128)(2,1)}), bf16[8,32,2]{1,2,0:T(2,128)(2,1)S(1)}, u32[]{:S(2)}, u32[]{:S(2)}) async-start(bf16[8,32,2]{1,2,0:T(2,128)(2,1)} %copy.28), calls=%async_computation.3 | async-start | bytes 8192 | tf_op jit(solution)/shard_map/all_to_all | solution.py:82
  109.1 0.2 fusion.2
  109.3 1.6 convolution_convert_fusion
  110.9 3.7 %all-to-all-done.3 = bf16[8,32,2]{1,2,0:T(2,128)(2,1)S(1)} async-done(((bf16[8,32,2]{1,2,0:T(2,128)(2,1)}), bf16[8,32,2]{1,2,0:T(2,128)(2,1)S(1)}, u32[]{:S(2)}, u32[]{:S(2)}) %all-to-all-start.3) | async-done | bytes 1056 | tf_op jit(solution)/shard_map/all_to_all | solution.py:82
  114.6 3.6 %all-to-all-start.4 = ((bf16[8,32,2048]{2,1,0:T(8,128)(2,1)}), bf16[8,32,2048]{2,1,0:T(8,128)(2,1)S(1)}, u32[]{:S(2)}, u32[]{:S(2)}) async-start(bf16[8,32,2048]{2,1,0:T(8,128)(2,1)} %bitcast.15), calls=%async_computation.4 | async-start | bytes 2097152 | tf_op jit(solution)/shard_map/all_to_all | solution.py:75
  118.3 0.3 mul.62
  118.6 0.2 copy.35
  118.8 25.8 %all-to-all-done.4 = bf16[8,32,2048]{2,1,0:T(8,128)(2,1)S(1)} async-done(((bf16[8,32,2048]{2,1,0:T(8,128)(2,1)}), bf16[8,32,2048]{2,1,0:T(8,128)(2,1)S(1)}, u32[]{:S(2)}, u32[]{:S(2)}) %all-to-all-start.4) | async-done | bytes 1048608 | tf_op jit(solution)/shard_map/all_to_all | solution.py:75
  144.6 4.6 %fusion.20 = f32[256,1024]{1,0:T(8,128)} fusion(bf16[256,2048]{1,0:T(8,128)(2,1)S(1)} %bitcast.77, bf16[1024,2048]{1,0:T(8,128)(2,1)} %bitcast.84), kind=kOutput, calls=%fused_computation.42 | convolution fusion | flops 1073741824 | bytes 6291456 | tf_op jit(solution)/shard_map/sd,hd->sh/dot_general | solution.py:34
  149.2 1.3 all-gather.8.cloned.1.call-done
  150.6 55.0 %all-gather.6.cloned.1.call-done = bf16[1,2,512,2048]{3,2,1,0:T(8,128)(2,1)} async-done(((bf16[1,2,128,2048]{3,2,1,0:T(8,128)(2,1)}), bf16[1,2,512,2048]{3,2,1,0:T(8,128)(2,1)}) %all-gather.6.cloned.1.call-update) | async-done | bytes 4194320 | tf_op jit(solution)/shard_map/all_gather | solution.py:94
  205.6 6.4 %convolution_convert_fusion.1 = bf16[256,2048]{1,0:T(8,128)(2,1)S(1)} fusion(bf16[1024,2048]{1,0:T(8,128)(2,1)} %bitcast.85, f32[256,1024]{1,0:T(8,128)S(1)} %bitcast.79, bf16[256,2048]{1,0:T(8,128)(2,1)S(1)} %bitcast.78, bf16[1024,2048]{1,0:T(8,128)(2,1)} %bitcast.86, f32[256,1024]{1,0:T(8,128)} %fusion.20), kind=kOutput, calls=%fused_computation.1 | convolution fusion | flops 2149842944 | bytes 12582912 | tf_op jit(solution)/shard_map/dot_general | solution.py:41
  212.0 31.0 %all_to_all.59 = bf16[8,32,2048]{2,1,0:T(8,128)(2,1)S(1)} all-to-all(bf16[8,32,2048]{2,1,0:T(8,128)(2,1)S(1)} %bitcast.80), channel_id=1, replica_groups=mesh['fs'=4,'tp'=8] {'tp'}, dimensions={0} | all-to-all | bytes 2097152 | tf_op jit(solution)/shard_map/all_to_all | solution.py:99
  243.0 1.1 convolution_convert_fusion.2
  (31 shorter events, 0.9 us)
Async XLA Ops:
  7.2 97.8 %copy-start = (bf16[128,2]{0,1:T(2,128)(2,1)S(1)}, bf16[128,2]{0,1:T(2,128)(2,1)}, u32[]{:S(2)}) copy-start(bf16[128,2]{0,1:T(2,128)(2,1)} %param.13) | copy-start | bytes 1540
  7.2 137.4 %all-gather.4.cloned.1.call-start = ((), (), s32[]{:S(2)}) async-start(), calls=%async_computation.6 | async-start | bytes 5242880 | tf_op jit(solution)/shard_map/all_gather | solution.py:93
  9.9 34.0 %copy-start.1 = (f32[8,2,128,256]{3,2,1,0:T(8,128)S(1)}, f32[8,2,128,256]{3,2,1,0:T(8,128)}, u32[]{:S(2)}) copy-start(f32[8,2,128,256]{3,2,1,0:T(8,128)} %param.11) | copy-start | bytes 6291460
  43.9 106.7 %all-gather.8.cloned.1.call-start = ((), (), s32[]{:S(2)}) async-start(), calls=%async_computation.8 | async-start | bytes 5242880 | tf_op jit(solution)/shard_map/all_gather | solution.py:95
  73.2 31.3 %copy-start.3 = (s32[128,1]{0,1:T(1,128)S(1)}, s32[128,1]{0,1:T(1,128)}, u32[]{:S(2)}) copy-start(s32[128,1]{0,1:T(1,128)} %param.12) | copy-start | bytes 1540
  73.2 35.9 %copy-start.2 = (bf16[128,2048]{1,0:T(8,128)(2,1)S(1)}, bf16[128,2048]{1,0:T(8,128)(2,1)}, u32[]{:S(2)}) copy-start(bf16[128,2048]{1,0:T(8,128)(2,1)} %param.7) | copy-start | bytes 1572868
  74.3 131.3 %all-gather.6.cloned.1.call-start = ((), (), s32[]{:S(2)}) async-start(), calls=%async_computation.7 | async-start | bytes 5242880 | tf_op jit(solution)/shard_map/all_gather | solution.py:94
  105.8 8.8 %all-to-all-start.3 = ((bf16[8,32,2]{1,2,0:T(2,128)(2,1)}), bf16[8,32,2]{1,2,0:T(2,128)(2,1)S(1)}, u32[]{:S(2)}, u32[]{:S(2)}) async-start(bf16[8,32,2]{1,2,0:T(2,128)(2,1)} %copy.28), calls=%async_computation.3 | async-start | bytes 8192 | tf_op jit(solution)/shard_map/all_to_all | solution.py:82
  114.6 30.1 %all-to-all-start.4 = ((bf16[8,32,2048]{2,1,0:T(8,128)(2,1)}), bf16[8,32,2048]{2,1,0:T(8,128)(2,1)S(1)}, u32[]{:S(2)}, u32[]{:S(2)}) async-start(bf16[8,32,2048]{2,1,0:T(8,128)(2,1)} %bitcast.15), calls=%async_computation.4 | async-start | bytes 2097152 | tf_op jit(solution)/shard_map/all_to_all | solution.py:75
Sparse Core Ops, SparseCore 0:
  44.0 51.4 all-gather.3
  98.0 52.5 all-gather.7
  153.0 52.5 all-gather.5
